TPU v7x, 32 devices: a whole 2x2x4 slice. The times are simulated.
32 devices in a mesh: ep: 8 (over z, y), tp: 4 (over x, core).
Axes of the slice: x: 2, y: 2, z: 4, core: 2. Of those that a mesh axis runs over, the one named last changes fastest.
Arguments:
- tokens: bfloat16 [192, 2048], P('ep'), may hold values from -6 to 6
- delta_state: float32 [192, 8, 128, 128], P('ep', 'tp'), may hold values from -3 to 3
- first_gain: bfloat16 [2048], replicated, may hold values from 0.099609375 to 1.8984375
- query_weight: bfloat16 [2048, 1024], P(None, 'tp'), may hold values from -0.125 to 0.125
- key_weight: bfloat16 [2048, 1024], P(None, 'tp'), may hold values from -0.125 to 0.125
- value_weight: bfloat16 [2048, 1024], P(None, 'tp'), may hold values from -0.125 to 0.125
- outgate_weight: bfloat16 [2048, 1024], P(None, 'tp'), may hold values from -0.125 to 0.125
- beta_weight: bfloat16 [2048, 8], replicated, may hold values from -0.125 to 0.125
- decay_weight: bfloat16 [2048, 8], replicated, may hold values from -0.125 to 0.125
- decay_rate: float32 [8], replicated, may hold values from 0.05 to 4
- decay_bias: float32 [8], replicated, may hold values from -3 to 3
- head_gain: bfloat16 [128], replicated, may hold values from 0.099609375 to 1.8984375
- out_weight: bfloat16 [1024, 2048], P('tp'), may hold values from -0.1875 to 0.1875
- second_gain: bfloat16 [2048], replicated, may hold values from 0.099609375 to 1.8984375
- blend_weight: bfloat16 [2048], replicated, may hold values from -0.125 to 0.125
- dense_gate_weight: bfloat16 [2048, 2048], P(None, 'tp'), may hold values from -0.125 to 0.125
- dense_up_weight: bfloat16 [2048, 2048], P(None, 'tp'), may hold values from -0.125 to 0.125
- dense_down_weight: bfloat16 [2048, 2048], P('tp'), may hold values from -0.125 to 0.125
- expert_gate: bfloat16 [32, 2048, 512], P(('ep', 'tp')), may hold values from -0.125 to 0.125
- expert_up: bfloat16 [32, 2048, 512], P(('ep', 'tp')), may hold values from -0.125 to 0.125
- expert_down: bfloat16 [32, 512, 2048], P(('ep', 'tp')), may hold values from -0.25 to 0.25
- route_ids: int32 [192, 6], P('ep'), may hold values from 0 to 31, all different within a row; in each aligned block of 24 rows (0 to 23, 24 to 47, ...) at most 7 rows name the same one
- route_weights: float32 [192, 6], P('ep'), may hold values from 0.1 to 1
Outputs:
- new_tokens: bfloat16 [192, 2048], P('ep')
- new_state: float32 [192, 8, 128, 128], P('ep', 'tp')
Inputs may be any that keep to these rules, and one draw needn't show every extreme that they name: `route_ids`: each row names 6 different experts. In each aligned block of 24 rows (the sequences of one index of ep) no expert is named by more than 7 rows, and in some block an expert is named by exactly 7 rows.
All inputs are finite; a program needn't handle non-finite values.
Results may differ from a plain program's by a relative error of at most 0.017.
Values may be sent and summed in bfloat16 or wider, within the bound.
A program may use at most 128 MiB of HBM per device.

v0:
```python
import jax
import jax.numpy as jnp
from jax import lax
from jax.sharding import PartitionSpec as P

norm_eps = 1e-06
unit_eps = 1e-06
routed_scale = 2.5


def rms_scale(values, gain):
    values = values.astype(jnp.float32)
    inverse = lax.rsqrt(jnp.mean(values * values, axis=-1, keepdims=True) + norm_eps)
    return values * inverse * gain.astype(jnp.float32)


def unit_rows(values):
    return values * lax.rsqrt(jnp.sum(values * values, axis=-1, keepdims=True) + unit_eps)


def rounded(values):
    return lax.optimization_barrier(values.astype(jnp.bfloat16)).astype(jnp.float32)


def delta_update(delta_state, query_raw, key_raw, value_raw, beta_gate, log_decay):
    head_size = delta_state.shape[-1]
    query_unit = unit_rows(jax.nn.silu(query_raw)) * head_size ** (-0.5)
    key_unit = unit_rows(jax.nn.silu(key_raw))
    value_act = jax.nn.silu(value_raw)
    decayed = jnp.exp(log_decay)[:, :, None, None] * delta_state
    predicted = jnp.einsum("shkv,shk->shv", decayed, key_unit, precision=lax.Precision.HIGHEST)
    update = (beta_gate[:, :, None] * key_unit)[:, :, :, None] * (value_act - predicted)[
        :, :, None, :
    ]
    new_state = decayed + update
    readout = jnp.einsum("shkv,shk->shv", new_state, query_unit, precision=lax.Precision.HIGHEST)
    return (new_state, readout)


def gated_heads(readout, outgate_raw, head_gain):
    scaled = rms_scale(readout, head_gain) * jax.nn.silu(outgate_raw)
    return scaled.reshape(scaled.shape[0], -1).astype(jnp.bfloat16)


def expert_rows(row_block, gate_mat, up_mat, down_mat):
    gate_part = jnp.dot(row_block, gate_mat, preferred_element_type=jnp.float32)
    up_part = jnp.dot(row_block, up_mat, preferred_element_type=jnp.float32)
    hidden = (jax.nn.silu(gate_part) * up_part).astype(jnp.bfloat16)
    return jnp.dot(hidden, down_mat, preferred_element_type=jnp.float32).astype(jnp.bfloat16)


def shards(
    tokens,
    delta_state,
    first_gain,
    query_weight,
    key_weight,
    value_weight,
    outgate_weight,
    beta_weight,
    decay_weight,
    decay_rate,
    decay_bias,
    head_gain,
    out_weight,
    second_gain,
    blend_weight,
    dense_gate_weight,
    dense_up_weight,
    dense_down_weight,
    expert_gate,
    expert_up,
    expert_down,
    route_ids,
    route_weights,
):
    seq_count = tokens.shape[0]
    head_local = delta_state.shape[1]
    head_size = delta_state.shape[2]
    top_count = route_ids.shape[1]
    ep_count = lax.axis_size("ep")
    tp_count = lax.axis_size("tp")
    tp_index = lax.axis_index("tp")
    normed = rms_scale(tokens, first_gain).astype(jnp.bfloat16)

    def project(weight):
        product = jnp.dot(normed, weight, preferred_element_type=jnp.float32)
        return rounded(product).reshape(seq_count, head_local, head_size)

    query_raw = project(query_weight)
    key_raw = project(key_weight)
    value_raw = project(value_weight)
    outgate_raw = project(outgate_weight)
    head_start = tp_index * head_local
    beta_all = jax.nn.sigmoid(jnp.dot(normed, beta_weight, preferred_element_type=jnp.float32))
    beta_gate = lax.dynamic_slice_in_dim(beta_all, head_start, head_local, 1)
    decay_input = jnp.dot(normed, decay_weight, preferred_element_type=jnp.float32) + decay_bias
    decay_all = -decay_rate * jax.nn.softplus(decay_input)
    log_decay = lax.dynamic_slice_in_dim(decay_all, head_start, head_local, 1)
    new_state, readout = delta_update(
        delta_state, query_raw, key_raw, value_raw, beta_gate, log_decay
    )
    gated = gated_heads(readout, outgate_raw, head_gain)
    mix_part = jnp.dot(gated, out_weight, preferred_element_type=jnp.float32)
    row_local = seq_count // tp_count
    mixed_rows = lax.psum_scatter(
        mix_part.astype(jnp.bfloat16), "tp", scatter_dimension=0, tiled=True
    ).astype(jnp.float32)
    own_tokens = lax.dynamic_slice_in_dim(tokens, tp_index * row_local, row_local, 0)
    residual_rows = (own_tokens.astype(jnp.float32) + mixed_rows).astype(jnp.bfloat16)
    normed_rows = rms_scale(residual_rows, second_gain).astype(jnp.bfloat16)
    normed_mid, residual = (
        lax.all_gather(normed_rows, "tp", axis=0, tiled=True),
        lax.all_gather(residual_rows, "tp", axis=0, tiled=True),
    )
    blend_gate = jax.nn.sigmoid(
        jnp.dot(normed_mid, blend_weight, preferred_element_type=jnp.float32)
    )
    dense_gate_raw = jnp.dot(normed_mid, dense_gate_weight, preferred_element_type=jnp.float32)
    dense_up_raw = jnp.dot(normed_mid, dense_up_weight, preferred_element_type=jnp.float32)
    dense_hidden = (jax.nn.silu(dense_gate_raw) * dense_up_raw).astype(jnp.bfloat16)
    dense_part = jnp.dot(dense_hidden, dense_down_weight, preferred_element_type=jnp.float32)
    expert_count = ep_count * tp_count
    capacity = max(2, (3 * seq_count * top_count + 2 * expert_count - 1) // (2 * expert_count))
    flat_ids = route_ids.reshape(-1)
    assign_count = flat_ids.shape[0]
    earlier = jnp.arange(assign_count)[:, None] > jnp.arange(assign_count)[None, :]
    matches = (flat_ids[:, None] == flat_ids[None, :]) & earlier
    rank_of = jnp.sum(matches.astype(jnp.int32), axis=1)
    owned = flat_ids % tp_count == tp_index
    slot_of = jnp.where(owned, flat_ids // tp_count * capacity + rank_of, -1)
    slot_total = ep_count * capacity
    slot_grid = slot_of.reshape(seq_count, top_count)
    slot_range = jnp.arange(slot_total, dtype=jnp.int32)
    dispatch = jnp.any(slot_grid[None, :, :] == slot_range[:, None, None], axis=2).astype(
        jnp.bfloat16
    )
    model_width = normed_mid.shape[1]
    outgoing = jnp.dot(dispatch, normed_mid, preferred_element_type=jnp.float32).astype(
        jnp.bfloat16
    )
    outgoing = outgoing.reshape(ep_count, capacity, model_width)
    arrived = lax.all_to_all(outgoing, "ep", split_axis=0, concat_axis=0, tiled=True)
    result = expert_rows(
        arrived.reshape(-1, model_width), expert_gate[0], expert_up[0], expert_down[0]
    )
    returned = lax.all_to_all(
        result.reshape(arrived.shape), "ep", split_axis=0, concat_axis=0, tiled=True
    )
    returned_rows = returned.reshape(slot_total, model_width)
    picked = returned_rows[jnp.maximum(slot_of, 0)].astype(jnp.float32)
    picked = picked.reshape(seq_count, top_count, model_width)
    route_scale = route_weights / jnp.sum(route_weights, axis=1, keepdims=True) * routed_scale
    kept_scale = jnp.where(owned.reshape(seq_count, top_count), route_scale, 0.0)
    routed_part = jnp.sum(kept_scale[:, :, None] * picked, axis=1)
    combined = lax.psum(
        (routed_part + blend_gate[:, None] * dense_part).astype(jnp.bfloat16), "tp"
    ).astype(jnp.float32)
    new_tokens = (residual.astype(jnp.float32) + combined).astype(jnp.bfloat16)
    return (new_tokens, new_state)


def solution(mesh):
    placed = (
        P("ep", None),
        P("ep", "tp", None, None),
        P(),
        P(None, "tp"),
        P(None, "tp"),
        P(None, "tp"),
        P(None, "tp"),
        P(),
        P(),
        P(),
        P(),
        P(),
        P("tp", None),
        P(),
        P(),
        P(None, "tp"),
        P(None, "tp"),
        P("tp", None),
        P(("ep", "tp"), None, None),
        P(("ep", "tp"), None, None),
        P(("ep", "tp"), None, None),
        P("ep", None),
        P("ep", None),
    )
    return jax.shard_map(
        shards,
        mesh=mesh,
        in_specs=placed,
        out_specs=(P("ep", None), P("ep", "tp", None, None)),
        check_vma=False,
    )
```

profile of v0, /device:TPU:0, one launch (start us, length us, event | category | flops | bytes accessed | tf_op | source)
XLA Modules:
  0.0 129.9 jit_solution(16252030878266203387)
XLA Ops:
  9.8 1.1 fusion.22
  10.9 1.2 fusion.59
  12.2 1.6 %convolution_convert_fusion.6 = bf16[24,256]{1,0:T(8,128)(2,1)S(1)} fusion(bf16[2048,256]{1,0:T(8,128)(2,1)} %param.27, bf16[24,2048]{1,0:T(8,128)(2,1)} %param.23, f32[2048]{0:T(1024)S(1)} %convert_element_type.92, f32[24]{0:T(128)S(1)} %add_rsqrt_fusion.4), kind=kOutput, calls=%fused_computation.24 | convolution fusion | flops 25368576 | bytes 1167456 | tf_op jit(solution)/shard_map/dot_general | solution.py:87
  14.0 1.6 %convolution_convert_fusion.5 = bf16[24,256]{1,0:T(8,128)(2,1)S(1)} fusion(bf16[2048,256]{1,0:T(8,128)(2,1)} %param.28, bf16[24,2048]{1,0:T(8,128)(2,1)} %param.23, f32[2048]{0:T(1024)S(1)} %convert_element_type.92, f32[24]{0:T(128)S(1)} %add_rsqrt_fusion.4), kind=kOutput, calls=%fused_computation.23 | convolution fusion | flops 25368576 | bytes 1167456 | tf_op jit(solution)/shard_map/dot_general | solution.py:87
  16.2 4.9 %fusion.1 = f32[24,2,1,128]{3,2,1,0:T(1,128)S(1)} fusion(f32[24,2,128,1]{2,3,1,0:T(1,128)S(1)} %bitcast.71, f32[24,2,128,128]{3,2,1,0:T(8,128)} %param.24, f32[24,2]{1,0:T(8,128)S(1)} %copy.47), kind=kOutput, calls=%fused_computation.2 | convolution fusion | flops 10223616 | bytes 3195072 | tf_op jit(solution)/shard_map/shkv,shk->shv/dot_general | solution.py:31
  21.2 1.1 multiply_add_fusion
  22.5 1.5 %copy-done.2 = f32[24,2,128,128]{3,2,1,0:T(8,128)} copy-done((f32[24,2,128,128]{3,2,1,0:T(8,128)}, f32[24,2,128,128]{3,2,1,0:T(8,128)S(1)}, u32[]{:S(2)}) %copy-start.2) | copy-done | bytes 3145752
  24.0 2.8 %fusion.69 = f32[24,2,1,128]{3,2,1,0:T(1,128)S(1)} fusion(f32[24,2,128,128]{3,2,1,0:T(8,128)S(1)} %multiply_add_fusion, f32[24,2,128,1]{2,3,1,0:T(1,128)S(1)} %bitcast.73), kind=kOutput, calls=%fused_computation.112 | convolution fusion | flops 9437184 | bytes 3194880 | tf_op jit(solution)/shard_map/shkv,shk->shv/dot_general | solution.py:36
  27.6 9.7 %fusion = bf16[8,2048]{1,0:T(8,128)(2,1)S(1)} fusion(bf16[24,2048]{1,0:T(8,128)(2,1)S(1)} %convolution_convert_fusion.2), kind=kCustom, calls=%all-reduce-scatter | all-reduce-scatter fusion | flops 65537 | bytes 131584
  37.3 1.3 collective-permute-start
  41.1 7.0 %all-gather.1 = bf16[4,6,2048]{2,1,0:T(8,128)(2,1)S(1)} all-gather(bf16[1,6,2048]{2,1,0:T(8,128)(2,1)S(1)} %fusion.46), channel_id=1, replica_groups=mesh['ep'=8,'tp'=4] {'tp'}, dimensions={0}, use_global_device_ids=true | all-gather | bytes 122880 | tf_op jit(solution)/shard_map/all_gather | solution.py:113
  49.2 5.8 %all-to-all-start = ((bf16[8,7,2048]{2,1,0:T(8,128)(2,1)}), bf16[8,7,2048]{2,1,0:T(8,128)(2,1)S(1)}, u32[]{:S(2)}, u32[]{:S(2)}) async-start(bf16[8,7,2048]{2,1,0:T(8,128)(2,1)} %reshape.269), calls=%async_computation | async-start | bytes 524288 | tf_op jit(solution)/shard_map/all_to_all | solution.py:143
  55.2 9.2 %all-to-all-done = bf16[8,7,2048]{2,1,0:T(8,128)(2,1)S(1)} async-done(((bf16[8,7,2048]{2,1,0:T(8,128)(2,1)}), bf16[8,7,2048]{2,1,0:T(8,128)(2,1)S(1)}, u32[]{:S(2)}, u32[]{:S(2)}) %all-to-all-start) | async-done | bytes 229408 | tf_op jit(solution)/shard_map/all_to_all | solution.py:143
  64.5 2.0 %fusion.8 = f32[56,512]{1,0:T(8,128)S(1)} fusion(bf16[56,2048]{1,0:T(8,128)(2,1)S(1)} %reshape.270, bf16[1,2048,512]{2,1,0:T(8,128)(2,1)} %param.41), kind=kOutput, calls=%fused_computation.13 | convolution fusion | flops 117440512 | bytes 2441216 | tf_op jit(solution)/shard_map/dot_general | solution.py:46
  66.6 2.5 %convolution_convert_fusion = bf16[56,2048]{1,0:T(8,128)(2,1)S(1)} fusion(bf16[1,512,2048]{2,1,0:T(8,128)(2,1)S(1)} %copy-done, bf16[56,2048]{1,0:T(8,128)(2,1)S(1)} %reshape.270, bf16[1,2048,512]{2,1,0:T(8,128)(2,1)} %param.42, f32[56,512]{1,0:T(8,128)S(1)} %fusion.8), kind=kOutput, calls=%fused_computation.4 | convolution fusion | flops 235167744 | bytes 4767744 | tf_op jit(solution)/shard_map/dot_general | solution.py:49
  69.8 3.6 %all-to-all-start.1 = ((bf16[8,7,2048]{2,1,0:T(8,128)(2,1)}), bf16[8,7,2048]{2,1,0:T(8,128)(2,1)S(1)}, u32[]{:S(2)}, u32[]{:S(2)}) async-start(bf16[8,7,2048]{2,1,0:T(8,128)(2,1)} %reshape.271), calls=%async_computation.1 | async-start | bytes 524288 | tf_op jit(solution)/shard_map/all_to_all | solution.py:147
  73.8 2.0 %fusion.70 = f32[24,512]{1,0:T(8,128)S(1)} fusion(bf16[24,2048]{1,0:T(8,128)(2,1)S(1)} %reshape.294, bf16[2048,512]{1,0:T(8,128)(2,1)} %param.38), kind=kOutput, calls=%fused_computation.113 | convolution fusion | flops 50331648 | bytes 2244608 | tf_op jit(solution)/shard_map/dot_general | solution.py:119
  75.8 6.6 %all-to-all-done.1 = bf16[8,7,2048]{2,1,0:T(8,128)(2,1)S(1)} async-done(((bf16[8,7,2048]{2,1,0:T(8,128)(2,1)}), bf16[8,7,2048]{2,1,0:T(8,128)(2,1)S(1)}, u32[]{:S(2)}, u32[]{:S(2)}) %all-to-all-start.1) | async-done | bytes 229408 | tf_op jit(solution)/shard_map/all_to_all | solution.py:147
  83.5 1.3 %reshape.282 = f32[24,6,2048]{2,1,0:T(8,128)} reshape(bf16[144,2048]{1,0:T(8,128)(2,1)S(1)} %gather_fusion) | data formatting | bytes 1769472 | tf_op jit(solution)/shard_map/convert_element_type | solution.py:151
  84.8 2.0 %multiply_reduce_fusion = f32[24,2048]{1,0:T(8,128)S(1)} fusion(f32[24,6,2048]{2,1,0:T(8,128)} %reshape.282, f32[24,6]{1,0:T(8,128)S(1)} %multiply_select_fusion), kind=kLoop, calls=%fused_computation.15 | loop fusion | flops 540672 | bytes 1376832 | tf_op jit(solution)/shard_map/reduce_sum | solution.py:155
  86.8 3.6 %fusion.4 = bf16[24,2048]{1,0:T(8,128)(2,1)} fusion(f32[24,2048]{1,0:T(8,128)S(1)} %multiply_reduce_fusion, bf16[512,2048]{1,0:T(8,128)(2,1)} %param.40, bf16[24,2048]{1,0:T(8,128)(2,1)S(1)} %reshape.294, bf16[2048,512]{1,0:T(8,128)(2,1)} %param.39, f32[24]{0:T(128)S(1)} %fusion.26, f32[24,512]{1,0:T(8,128)S(1)} %fusion.70), kind=kOutput, calls=%fused_computation.8 | convolution fusion | flops 100884480 | bytes 4636768 | tf_op jit(solution)/shard_map/dot_general | solution.py:122
  90.4 5.4 %all-gather = bf16[4,6,2048]{2,1,0:T(8,128)(2,1)S(1)} all-gather(bf16[1,6,2048]{2,1,0:T(8,128)(2,1)S(1)} %bitcast.68), channel_id=1, replica_groups=mesh['ep'=8,'tp'=4] {'tp'}, dimensions={0}, use_global_device_ids=true | all-gather | bytes 122880 | tf_op jit(solution)/shard_map/all_gather | solution.py:114
  95.9 25.7 %all-reduce.4.cloned.1.call-done = bf16[24,2048]{1,0:T(8,128)(2,1)} async-done(((bf16[24,2048]{1,0:T(8,128)(2,1)}), bf16[24,2048]{1,0:T(8,128)(2,1)}) %all-reduce.4.cloned.1.call-update) | async-done | bytes 98320 | tf_op jit(solution)/shard_map/psum | solution.py:156
  121.5 1.6 %add_convert_fusion = bf16[24,2048]{1,0:T(8,128)(2,1)} fusion(f32[24,2048]{1,0:T(8,128)S(1)} %reshape.295, bf16[24,2048]{1,0:T(8,128)(2,1)} %all-reduce.4.cloned.1.call-done), kind=kLoop, calls=%fused_computation.40 | loop fusion | flops 147456 | bytes 393216 | tf_op jit(solution)/shard_map/convert_element_type | solution.py:159
  (83 shorter events, 9.9 us)
Async XLA Ops:
  7.2 59.4 %copy-start = (bf16[1,512,2048]{2,1,0:T(8,128)(2,1)S(1)}, bf16[1,512,2048]{2,1,0:T(8,128)(2,1)}, u32[]{:S(2)}) copy-start(bf16[1,512,2048]{2,1,0:T(8,128)(2,1)} %param.43) | copy-start | bytes 6291460
  7.2 8.4 %copy-start.3 = (bf16[24,2048]{1,0:T(8,128)(2,1)S(1)}, bf16[24,2048]{1,0:T(8,128)(2,1)}, u32[]{:S(2)}) copy-start(bf16[24,2048]{1,0:T(8,128)(2,1)} %param.23) | copy-start | bytes 294916
  7.2 8.4 %copy-start.4 = (bf16[2048,256]{1,0:T(8,128)(2,1)S(1)}, bf16[2048,256]{1,0:T(8,128)(2,1)}, u32[]{:S(2)}) copy-start(bf16[2048,256]{1,0:T(8,128)(2,1)} %param.26) | copy-start | bytes 3145732
  16.0 5.3 %copy-start.1 = (f32[24,2,128,128]{3,2,1,0:T(8,128)S(1)}, f32[24,2,128,128]{3,2,1,0:T(8,128)}, u32[]{:S(2)}) copy-start(f32[24,2,128,128]{3,2,1,0:T(8,128)} %param.24) | copy-start | bytes 9437188
  22.3 1.7 %copy-start.2 = (f32[24,2,128,128]{3,2,1,0:T(8,128)}, f32[24,2,128,128]{3,2,1,0:T(8,128)S(1)}, u32[]{:S(2)}) copy-start(f32[24,2,128,128]{3,2,1,0:T(8,128)S(1)} %multiply_add_fusion) | copy-start | bytes 9437188
  22.4 4.6 %copy-start.5 = (bf16[2048,256]{1,0:T(8,128)(2,1)S(1)}, bf16[2048,256]{1,0:T(8,128)(2,1)}, u32[]{:S(2)}) copy-start(bf16[2048,256]{1,0:T(8,128)(2,1)} %param.29) | copy-start | bytes 3145732
  24.0 3.3 %copy-start.12 = (bf16[128]{0:T(256)(128)(2,1)S(1)}, bf16[128]{0:T(256)(128)(2,1)}, u32[]{:S(2)}) copy-start(bf16[128]{0:T(256)(128)(2,1)} %param.34) | copy-start | bytes 772
  24.0 3.4 %copy-start.6 = (bf16[256,2048]{1,0:T(8,128)(2,1)S(1)}, bf16[256,2048]{1,0:T(8,128)(2,1)}, u32[]{:S(2)}) copy-start(bf16[256,2048]{1,0:T(8,128)(2,1)} %param.35) | copy-start | bytes 3145732
  26.8 11.8 %copy-start.10 = (s32[24,6]{0,1:T(8,128)S(1)}, s32[24,6]{0,1:T(8,128)}, u32[]{:S(2)}) copy-start(s32[24,6]{0,1:T(8,128)} %param.44) | copy-start | bytes 1732
  26.8 12.6 %copy-start.8 = (bf16[2048]{0:T(1024)(128)(2,1)S(1)}, bf16[2048]{0:T(1024)(128)(2,1)}, u32[]{:S(2)}) copy-start(bf16[2048]{0:T(1024)(128)(2,1)} %param.36) | copy-start | bytes 12292
  26.8 12.7 %copy-start.11 = (u32[32]{0:T(128)S(1)}, u32[32]{0:T(128)}, u32[]{:S(2)}) copy-start(u32[32]{0:T(128)} %constant.90) | copy-start | bytes 388
  27.2 27.8 %copy-start.7 = (f32[24,6]{0,1:T(8,128)S(1)}, f32[24,6]{0,1:T(8,128)}, u32[]{:S(2)}) copy-start(f32[24,6]{0,1:T(8,128)} %param.45) | copy-start | bytes 1732
  27.2 27.9 %copy-start.9 = (bf16[2048]{0:T(1024)(128)(2,1)S(1)}, bf16[2048]{0:T(1024)(128)(2,1)}, u32[]{:S(2)}) copy-start(bf16[2048]{0:T(1024)(128)(2,1)} %param.37) | copy-start | bytes 12292
  37.3 3.4 %collective-permute-start = (bf16[6,2048]{1,0:T(8,128)(2,1)S(1)}, bf16[6,2048]{1,0:T(8,128)(2,1)S(1)}, u32[]{:S(2)}, u32[]{:S(2)}) collective-permute-start(bf16[6,2048]{1,0:T(8,128)(2,1)S(1)} %slice.2), channel_id=1, source_target_pairs={{0,1},{1,2},{2,3},{4,5},{5,6},{6,7},{8,9},{9,10},{10,11},{12,13},{... | collective-permute-start | bytes 73736
  49.2 15.3 %all-to-all-start = ((bf16[8,7,2048]{2,1,0:T(8,128)(2,1)}), bf16[8,7,2048]{2,1,0:T(8,128)(2,1)S(1)}, u32[]{:S(2)}, u32[]{:S(2)}) async-start(bf16[8,7,2048]{2,1,0:T(8,128)(2,1)} %reshape.269), calls=%async_computation | async-start | bytes 524288 | tf_op jit(solution)/shard_map/all_to_all | solution.py:143
  69.8 12.6 %all-to-all-start.1 = ((bf16[8,7,2048]{2,1,0:T(8,128)(2,1)}), bf16[8,7,2048]{2,1,0:T(8,128)(2,1)S(1)}, u32[]{:S(2)}, u32[]{:S(2)}) async-start(bf16[8,7,2048]{2,1,0:T(8,128)(2,1)} %reshape.271), calls=%async_computation.1 | async-start | bytes 524288 | tf_op jit(solution)/shard_map/all_to_all | solution.py:147
  73.4 48.1 %all-reduce.4.cloned.1.call-start = ((), (), s32[]{:S(2)}) async-start(), calls=%async_computation.2 | async-start | bytes 196608 | tf_op jit(solution)/shard_map/psum | solution.py:156
Sparse Core Ops, SparseCore 0:
  90.5 30.9 all-reduce.3
where the time goes:
time: 131 us; the launch traced here: 130 us
  waiting for transfers between devices  41.5 us (32%)
  matrix products  24.5 us (19%)
  blocking collectives  22 us (17%)
  between operations  15.1 us (12%)
  starting transfers between devices  10.9 us (8%)
  other arithmetic  8.59 us (7%)
  local copies, waits for them, and re-layouts  7.27 us (6%)
    psum x1, waiting for transfers between devices, shards(): lax.psum((routed_part + blend_gate[:, None] * dense_part).astype(jnp.bflo...  25.7 us
    unnamed x1, blocking collectives  9.66 us
    all_to_all x1, waiting for transfers between devices, shards(): lax.all_to_all(outgoing, 'ep', split_axis=0, concat_axis=0, tiled=True)  9.18 us
    all_gather x1, blocking collectives, shards(): lax.all_gather(normed_rows, 'tp', axis=0, tiled=True)  6.97 us
    all_to_all x1, waiting for transfers between devices, shards(): lax.all_to_all(result.reshape(arrived.shape), 'ep', split_axis=0, concat_...  6.63 us
    all_to_all x1, starting transfers between devices, shards(): lax.all_to_all(outgoing, 'ep', split_axis=0, concat_axis=0, tiled=True)  5.83 us
    all_gather x1, blocking collectives, shards(): lax.all_gather(residual_rows, 'tp', axis=0, tiled=True)  5.42 us
    dot_general x1, matrix products, delta_update(): jnp.einsum('shkv,shk->shv', decayed, key_unit, precision=lax.Precision.HI...  4.94 us
  transfers between devices with their start and end apart: 4, of which 3 were waited for; matrix products, arithmetic and copies ran while one was open for 3% of the time, Pallas kernels for 0%

commit v1 on v0

--- a/solution.py
+++ b/solution.py
@@ -153,8 +153,9 @@
     route_scale = route_weights / jnp.sum(route_weights, axis=1, keepdims=True) * routed_scale
     kept_scale = jnp.where(owned.reshape(seq_count, top_count), route_scale, 0.0)
     routed_part = jnp.sum(kept_scale[:, :, None] * picked, axis=1)
-    combined = lax.psum(
-        (routed_part + blend_gate[:, None] * dense_part).astype(jnp.bfloat16), "tp"
+    combined = jnp.sum(
+        lax.all_gather((routed_part + blend_gate[:, None] * dense_part).astype(jnp.bfloat16), "tp"),
+        axis=0,
     ).astype(jnp.float32)
     new_tokens = (residual.astype(jnp.float32) + combined).astype(jnp.bfloat16)
     return (new_tokens, new_state)

time: 131 us -> 91.3 us (0.70)
  waiting for transfers between devices: 41.5 us -> 10.6 us
  between operations: 15.1 us -> 1.73 us
  blocking collectives: 22 us -> 28.7 us
    psum x1 -> x0, waiting for transfers between devices: 25.7 us -> none  [shards(): lax.psum((routed_part + blend_gate[:, None] * dense_part).astype(jnp.bflo...]
    all_gather x0 -> x1, blocking collectives: none -> 6.71 us  [shards(): lax.all_gather((routed_part + blend_gate[:, None] * dense_part).astype(jn...]
    all_to_all x1, waiting for transfers between devices: 9.18 us -> 3.74 us  [shards(): lax.all_to_all(outgoing, 'ep', split_axis=0, concat_axis=0, tiled=True)]
  transfers between devices with their start and end apart: 4 -> 3, of which waited for: 3 -> 2; matrix products, arithmetic and copies ran while one was open for 3% -> 4% of each run, Pallas kernels for 0% -> 0%
where the time goes in v1:
time: 91.3 us; the launch traced here: 90.7 us
  blocking collectives  28.7 us (31%)
  matrix products  23.9 us (26%)
  starting transfers between devices  10.7 us (12%)
  waiting for transfers between devices  10.6 us (12%)
  other arithmetic  7.76 us (8%)
  local copies, waits for them, and re-layouts  7.27 us (8%)
  between operations  1.73 us (2%)
    unnamed x1, blocking collectives  9.66 us
    all_gather x1, blocking collectives, shards(): lax.all_gather(normed_rows, 'tp', axis=0, tiled=True)  6.97 us
    all_to_all x1, waiting for transfers between devices, shards(): lax.all_to_all(result.reshape(arrived.shape), 'ep', split_axis=0, concat_...  6.86 us
    all_gather x1, blocking collectives, shards(): lax.all_gather((routed_part + blend_gate[:, None] * dense_part).astype(jn...  6.71 us
    all_to_all x1, starting transfers between devices, shards(): lax.all_to_all(outgoing, 'ep', split_axis=0, concat_axis=0, tiled=True)  5.83 us
    all_gather x1, blocking collectives, shards(): lax.all_gather(residual_rows, 'tp', axis=0, tiled=True)  5.4 us
    dot_general x1, matrix products, delta_update(): jnp.einsum('shkv,shk->shv', decayed, key_unit, precision=lax.Precision.HI...  4.94 us
    all_to_all x1, waiting for transfers between devices, shards(): lax.all_to_all(outgoing, 'ep', split_axis=0, concat_axis=0, tiled=True)  3.74 us
  transfers between devices with their start and end apart: 3, of which 2 were waited for; matrix products, arithmetic and copies ran while one was open for 4% of the time, Pallas kernels for 0%

profile of v1, /device:TPU:0, one launch (start us, length us, event | category | flops | bytes accessed | tf_op | source)
XLA Modules:
  0.0 90.7 jit_solution(17125129964318420340)
XLA Ops:
  1.5 1.1 %fusion.27 = f32[24]{0:T(128)S(1)} fusion(bf16[24,2048]{1,0:T(8,128)(2,1)} %param.23), kind=kLoop, calls=%fused_computation.37 | loop fusion | flops 147432 | bytes 98400 | tf_op jit(solution)/shard_map/reduce_sum | solution.py:13
  3.3 1.1 %fusion.22 = f32[24,8]{0,1:T(8,128)S(1)} fusion(bf16[2048,8]{0,1:T(8,128)(2,1)} %param.30, bf16[24,2048]{1,0:T(8,128)(2,1)} %param.23, f32[2048]{0:T(1024)S(1)} %convert_element_type.94, f32[24]{0:T(128)S(1)} %add_rsqrt_fusion.4), kind=kOutput, calls=%fused_computation.28 | convolution fusion | flops 983616 | bytes 140128 | tf_op jit(solution)/shard_map/dot_general | solution.py:95
  4.4 1.2 %fusion.59 = f32[24,8]{0,1:T(8,128)S(1)} fusion(bf16[2048,8]{0,1:T(8,128)(2,1)} %param.31, f32[8]{0:T(128)} %param.33, f32[8]{0:T(128)S(1)} %neg.38, bf16[24,2048]{1,0:T(8,128)(2,1)} %param.23, f32[2048]{0:T(1024)S(1)} %convert_element_type.94, f32[24]{0:T(128)S(1)} %add_rsqrt_fusion.4), kind=kOutput, calls=%fused_computation.97 | convolution fusion | flops 984576 | bytes 140192 | tf_op jit(solution)/shard_map/dot_general | solution.py:97
  5.6 1.6 %convolution_convert_fusion.6 = bf16[24,256]{1,0:T(8,128)(2,1)S(1)} fusion(bf16[2048,256]{1,0:T(8,128)(2,1)} %param.27, bf16[24,2048]{1,0:T(8,128)(2,1)} %param.23, f32[2048]{0:T(1024)S(1)} %convert_element_type.94, f32[24]{0:T(128)S(1)} %add_rsqrt_fusion.4), kind=kOutput, calls=%fused_computation.24 | convolution fusion | flops 25368576 | bytes 1167456 | tf_op jit(solution)/shard_map/dot_general | solution.py:87
  7.5 1.6 %convolution_convert_fusion.5 = bf16[24,256]{1,0:T(8,128)(2,1)S(1)} fusion(bf16[2048,256]{1,0:T(8,128)(2,1)} %param.28, bf16[24,2048]{1,0:T(8,128)(2,1)} %param.23, f32[2048]{0:T(1024)S(1)} %convert_element_type.94, f32[24]{0:T(128)S(1)} %add_rsqrt_fusion.4), kind=kOutput, calls=%fused_computation.23 | convolution fusion | flops 25368576 | bytes 1167456 | tf_op jit(solution)/shard_map/dot_general | solution.py:87
  9.7 4.9 %fusion.1 = f32[24,2,1,128]{3,2,1,0:T(1,128)S(1)} fusion(f32[24,2,128,1]{2,3,1,0:T(1,128)S(1)} %bitcast.73, f32[24,2,128,128]{3,2,1,0:T(8,128)} %param.24, f32[24,2]{1,0:T(8,128)S(1)} %copy.47), kind=kOutput, calls=%fused_computation.2 | convolution fusion | flops 10223616 | bytes 3195072 | tf_op jit(solution)/shard_map/shkv,shk->shv/dot_general | solution.py:31
  14.7 1.1 %multiply_add_fusion = f32[24,2,128,128]{3,2,1,0:T(8,128)S(1)} fusion(f32[24,2,128,128]{3,2,1,0:T(8,128)S(1)} %copy-done.1, f32[24,2,128]{2,1,0:T(2,128)S(1)} %fusion.47, f32[24,2,128]{2,1,0:T(2,128)S(1)} %get-tuple-element.6, f32[24,2]{1,0:T(8,128)S(1)} %copy.47), kind=kLoop, calls=%fused_computation.1 | loop fusion | flops 2359296 | bytes 6340800 | tf_op jit(solution)/shard_map/add | solution.py:35
  15.9 1.5 %copy-done.2 = f32[24,2,128,128]{3,2,1,0:T(8,128)} copy-done((f32[24,2,128,128]{3,2,1,0:T(8,128)}, f32[24,2,128,128]{3,2,1,0:T(8,128)S(1)}, u32[]{:S(2)}) %copy-start.2) | copy-done | bytes 3145752
  17.5 2.8 %fusion.69 = f32[24,2,1,128]{3,2,1,0:T(1,128)S(1)} fusion(f32[24,2,128,128]{3,2,1,0:T(8,128)S(1)} %multiply_add_fusion, f32[24,2,128,1]{2,3,1,0:T(1,128)S(1)} %bitcast.75), kind=kOutput, calls=%fused_computation.112 | convolution fusion | flops 9437184 | bytes 3194880 | tf_op jit(solution)/shard_map/shkv,shk->shv/dot_general | solution.py:36
  21.1 9.7 %fusion = bf16[8,2048]{1,0:T(8,128)(2,1)S(1)} fusion(bf16[24,2048]{1,0:T(8,128)(2,1)S(1)} %convolution_convert_fusion.2), kind=kCustom, calls=%all-reduce-scatter | all-reduce-scatter fusion | flops 65537 | bytes 131584
  30.8 1.3 %collective-permute-start = (bf16[6,2048]{1,0:T(8,128)(2,1)S(1)}, bf16[6,2048]{1,0:T(8,128)(2,1)S(1)}, u32[]{:S(2)}, u32[]{:S(2)}) collective-permute-start(bf16[6,2048]{1,0:T(8,128)(2,1)S(1)} %slice.2), channel_id=1, source_target_pairs={{0,1},{1,2},{2,3},{4,5},{5,6},{6,7},{8,9},{9,10},{10,11},{12,13},{... | collective-permute-start | bytes 73736
  34.6 7.0 %all-gather.2 = bf16[4,6,2048]{2,1,0:T(8,128)(2,1)S(1)} all-gather(bf16[1,6,2048]{2,1,0:T(8,128)(2,1)S(1)} %fusion.46), channel_id=1, replica_groups=mesh['ep'=8,'tp'=4] {'tp'}, dimensions={0}, use_global_device_ids=true | all-gather | bytes 122880 | tf_op jit(solution)/shard_map/all_gather | solution.py:113
  42.6 5.8 %all-to-all-start = ((bf16[8,7,2048]{2,1,0:T(8,128)(2,1)}), bf16[8,7,2048]{2,1,0:T(8,128)(2,1)S(1)}, u32[]{:S(2)}, u32[]{:S(2)}) async-start(bf16[8,7,2048]{2,1,0:T(8,128)(2,1)} %reshape.269), calls=%async_computation | async-start | bytes 524288 | tf_op jit(solution)/shard_map/all_to_all | solution.py:143
  48.7 5.4 %all-gather.1 = bf16[4,6,2048]{2,1,0:T(8,128)(2,1)S(1)} all-gather(bf16[1,6,2048]{2,1,0:T(8,128)(2,1)S(1)} %bitcast.70), channel_id=1, replica_groups=mesh['ep'=8,'tp'=4] {'tp'}, dimensions={0}, use_global_device_ids=true | all-gather | bytes 122880 | tf_op jit(solution)/shard_map/all_gather | solution.py:114
  54.1 3.7 %all-to-all-done = bf16[8,7,2048]{2,1,0:T(8,128)(2,1)S(1)} async-done(((bf16[8,7,2048]{2,1,0:T(8,128)(2,1)}), bf16[8,7,2048]{2,1,0:T(8,128)(2,1)S(1)}, u32[]{:S(2)}, u32[]{:S(2)}) %all-to-all-start) | async-done | bytes 229408 | tf_op jit(solution)/shard_map/all_to_all | solution.py:143
  58.0 2.0 %fusion.8 = f32[56,512]{1,0:T(8,128)S(1)} fusion(bf16[56,2048]{1,0:T(8,128)(2,1)S(1)} %reshape.270, bf16[1,2048,512]{2,1,0:T(8,128)(2,1)} %param.41), kind=kOutput, calls=%fused_computation.13 | convolution fusion | flops 117440512 | bytes 2441216 | tf_op jit(solution)/shard_map/dot_general | solution.py:46
  60.0 2.5 %convolution_convert_fusion = bf16[56,2048]{1,0:T(8,128)(2,1)S(1)} fusion(bf16[1,512,2048]{2,1,0:T(8,128)(2,1)S(1)} %copy-done, bf16[56,2048]{1,0:T(8,128)(2,1)S(1)} %reshape.270, bf16[1,2048,512]{2,1,0:T(8,128)(2,1)} %param.42, f32[56,512]{1,0:T(8,128)S(1)} %fusion.8), kind=kOutput, calls=%fused_computation.4 | convolution fusion | flops 235167744 | bytes 4767744 | tf_op jit(solution)/shard_map/dot_general | solution.py:49
  63.3 3.6 %all-to-all-start.1 = ((bf16[8,7,2048]{2,1,0:T(8,128)(2,1)}), bf16[8,7,2048]{2,1,0:T(8,128)(2,1)S(1)}, u32[]{:S(2)}, u32[]{:S(2)}) async-start(bf16[8,7,2048]{2,1,0:T(8,128)(2,1)} %reshape.271), calls=%async_computation.1 | async-start | bytes 524288 | tf_op jit(solution)/shard_map/all_to_all | solution.py:147
  67.0 2.0 %fusion.70 = f32[24,512]{1,0:T(8,128)S(1)} fusion(bf16[24,2048]{1,0:T(8,128)(2,1)S(1)} %reshape.295, bf16[2048,512]{1,0:T(8,128)(2,1)} %param.38), kind=kOutput, calls=%fused_computation.113 | convolution fusion | flops 50331648 | bytes 2244608 | tf_op jit(solution)/shard_map/dot_general | solution.py:119
  69.0 6.9 %all-to-all-done.1 = bf16[8,7,2048]{2,1,0:T(8,128)(2,1)S(1)} async-done(((bf16[8,7,2048]{2,1,0:T(8,128)(2,1)}), bf16[8,7,2048]{2,1,0:T(8,128)(2,1)S(1)}, u32[]{:S(2)}, u32[]{:S(2)}) %all-to-all-start.1) | async-done | bytes 229408 | tf_op jit(solution)/shard_map/all_to_all | solution.py:147
  77.0 1.3 %reshape.282 = f32[24,6,2048]{2,1,0:T(8,128)} reshape(bf16[144,2048]{1,0:T(8,128)(2,1)S(1)} %gather_fusion) | data formatting | bytes 1769472 | tf_op jit(solution)/shard_map/convert_element_type | solution.py:151
  78.3 2.0 %multiply_reduce_fusion = f32[24,2048]{1,0:T(8,128)S(1)} fusion(f32[24,6,2048]{2,1,0:T(8,128)} %reshape.282, f32[24,6]{1,0:T(8,128)S(1)} %multiply_select_fusion), kind=kLoop, calls=%fused_computation.15 | loop fusion | flops 540672 | bytes 1376832 | tf_op jit(solution)/shard_map/reduce_sum | solution.py:155
  80.2 3.0 %fusion.4 = bf16[24,2048]{1,0:T(8,128)(2,1)S(1)} fusion(f32[24,2048]{1,0:T(8,128)S(1)} %multiply_reduce_fusion, bf16[512,2048]{1,0:T(8,128)(2,1)} %param.40, bf16[24,2048]{1,0:T(8,128)(2,1)S(1)} %reshape.295, bf16[2048,512]{1,0:T(8,128)(2,1)} %param.39, f32[24]{0:T(128)S(1)} %fusion.26, f32[24,512]{1,0:T(8,128)S(1)} %fusion.70), kind=kOutput, calls=%fused_computation.8 | convolution fusion | flops 100884480 | bytes 4636768 | tf_op jit(solution)/shard_map/dot_general | solution.py:122
  83.2 6.7 %all-gather = bf16[96,2048]{1,0:T(8,128)(2,1)S(1)} all-gather(bf16[24,2048]{1,0:T(8,128)(2,1)S(1)} %fusion.4), channel_id=2, replica_groups=mesh['ep'=8,'tp'=4] {'tp'}, dimensions={0}, use_global_device_ids=true | all-gather | bytes 491520 | tf_op jit(solution)/shard_map/all_gather | solution.py:157
  (82 shorter events, 9.3 us)
Async XLA Ops:
  0.6 59.4 %copy-start = (bf16[1,512,2048]{2,1,0:T(8,128)(2,1)S(1)}, bf16[1,512,2048]{2,1,0:T(8,128)(2,1)}, u32[]{:S(2)}) copy-start(bf16[1,512,2048]{2,1,0:T(8,128)(2,1)} %param.43) | copy-start | bytes 6291460
  0.6 8.4 %copy-start.3 = (bf16[24,2048]{1,0:T(8,128)(2,1)S(1)}, bf16[24,2048]{1,0:T(8,128)(2,1)}, u32[]{:S(2)}) copy-start(bf16[24,2048]{1,0:T(8,128)(2,1)} %param.23) | copy-start | bytes 294916
  0.7 8.4 %copy-start.4 = (bf16[2048,256]{1,0:T(8,128)(2,1)S(1)}, bf16[2048,256]{1,0:T(8,128)(2,1)}, u32[]{:S(2)}) copy-start(bf16[2048,256]{1,0:T(8,128)(2,1)} %param.26) | copy-start | bytes 3145732
  9.4 5.3 %copy-start.1 = (f32[24,2,128,128]{3,2,1,0:T(8,128)S(1)}, f32[24,2,128,128]{3,2,1,0:T(8,128)}, u32[]{:S(2)}) copy-start(f32[24,2,128,128]{3,2,1,0:T(8,128)} %param.24) | copy-start | bytes 9437188
  15.8 1.7 %copy-start.2 = (f32[24,2,128,128]{3,2,1,0:T(8,128)}, f32[24,2,128,128]{3,2,1,0:T(8,128)S(1)}, u32[]{:S(2)}) copy-start(f32[24,2,128,128]{3,2,1,0:T(8,128)S(1)} %multiply_add_fusion) | copy-start | bytes 9437188
  15.8 4.6 %copy-start.5 = (bf16[2048,256]{1,0:T(8,128)(2,1)S(1)}, bf16[2048,256]{1,0:T(8,128)(2,1)}, u32[]{:S(2)}) copy-start(bf16[2048,256]{1,0:T(8,128)(2,1)} %param.29) | copy-start | bytes 3145732
  17.5 3.3 %copy-start.12 = (bf16[128]{0:T(256)(128)(2,1)S(1)}, bf16[128]{0:T(256)(128)(2,1)}, u32[]{:S(2)}) copy-start(bf16[128]{0:T(256)(128)(2,1)} %param.34) | copy-start | bytes 772
  17.5 3.4 %copy-start.6 = (bf16[256,2048]{1,0:T(8,128)(2,1)S(1)}, bf16[256,2048]{1,0:T(8,128)(2,1)}, u32[]{:S(2)}) copy-start(bf16[256,2048]{1,0:T(8,128)(2,1)} %param.35) | copy-start | bytes 3145732
  20.2 11.8 %copy-start.10 = (s32[24,6]{0,1:T(8,128)S(1)}, s32[24,6]{0,1:T(8,128)}, u32[]{:S(2)}) copy-start(s32[24,6]{0,1:T(8,128)} %param.44) | copy-start | bytes 1732
  20.3 12.6 %copy-start.8 = (bf16[2048]{0:T(1024)(128)(2,1)S(1)}, bf16[2048]{0:T(1024)(128)(2,1)}, u32[]{:S(2)}) copy-start(bf16[2048]{0:T(1024)(128)(2,1)} %param.36) | copy-start | bytes 12292
  20.3 12.7 %copy-start.11 = (u32[32]{0:T(128)S(1)}, u32[32]{0:T(128)}, u32[]{:S(2)}) copy-start(u32[32]{0:T(128)} %constant.92) | copy-start | bytes 388
  20.7 27.8 %copy-start.7 = (f32[24,6]{0,1:T(8,128)S(1)}, f32[24,6]{0,1:T(8,128)}, u32[]{:S(2)}) copy-start(f32[24,6]{0,1:T(8,128)} %param.45) | copy-start | bytes 1732
  20.7 27.9 %copy-start.9 = (bf16[2048]{0:T(1024)(128)(2,1)S(1)}, bf16[2048]{0:T(1024)(128)(2,1)}, u32[]{:S(2)}) copy-start(bf16[2048]{0:T(1024)(128)(2,1)} %param.37) | copy-start | bytes 12292
  30.8 3.4 %collective-permute-start = (bf16[6,2048]{1,0:T(8,128)(2,1)S(1)}, bf16[6,2048]{1,0:T(8,128)(2,1)S(1)}, u32[]{:S(2)}, u32[]{:S(2)}) collective-permute-start(bf16[6,2048]{1,0:T(8,128)(2,1)S(1)} %slice.2), channel_id=1, source_target_pairs={{0,1},{1,2},{2,3},{4,5},{5,6},{6,7},{8,9},{9,10},{10,11},{12,13},{... | collective-permute-start | bytes 73736
  42.6 15.3 %all-to-all-start = ((bf16[8,7,2048]{2,1,0:T(8,128)(2,1)}), bf16[8,7,2048]{2,1,0:T(8,128)(2,1)S(1)}, u32[]{:S(2)}, u32[]{:S(2)}) async-start(bf16[8,7,2048]{2,1,0:T(8,128)(2,1)} %reshape.269), calls=%async_computation | async-start | bytes 524288 | tf_op jit(solution)/shard_map/all_to_all | solution.py:143
  63.3 12.6 %all-to-all-start.1 = ((bf16[8,7,2048]{2,1,0:T(8,128)(2,1)}), bf16[8,7,2048]{2,1,0:T(8,128)(2,1)S(1)}, u32[]{:S(2)}, u32[]{:S(2)}) async-start(bf16[8,7,2048]{2,1,0:T(8,128)(2,1)} %reshape.271), calls=%async_computation.1 | async-start | bytes 524288 | tf_op jit(solution)/shard_map/all_to_all | solution.py:147
